TPU v7x, 32 devices: a whole 2x2x4 slice. The times are simulated.
32 devices in a mesh: sp: 8 (over z, x), tp: 4 (over y, core).
Axes of the slice: x: 2, y: 2, z: 4, core: 2. Of those that a mesh axis runs over, the one named last changes fastest.
Arguments:
- residual: bfloat16 [6144, 2048], P('sp'), may hold values from -6 to 6
- query_matrix: bfloat16 [6144, 1024], P('sp', 'tp'), may hold values from -6 to 6
- key_matrix: bfloat16 [6144, 1024], P('sp', 'tp'), may hold values from -6 to 6
- value_matrix: bfloat16 [6144, 2048], P('sp', 'tp'), may hold values from -6 to 6
- output_gate_logit: bfloat16 [6144, 2048], P('sp', 'tp'), may hold values from -6 to 6
- input_gate_log: float32 [6144, 8], P('sp', 'tp'), may hold values from -4 to 125
- forget_gate_logit: float32 [6144, 8], P('sp', 'tp')
- extra_head_decay: float32 [6144, 8], P('sp', 'tp'), may hold values from -1 to 0
- head_norm_gain: float32 [2048], P('tp'), may hold values from 0.1 to 1.9
- projection: bfloat16 [2048, 2048], P('tp'), may hold values from -5.303301 to 5.303301
- cell_output_gain: float32 [2048], replicated, may hold values from 0.1 to 1.9
- mixer_input_gain: float32 [2048], replicated, may hold values from 0.1 to 1.9
- mixer_gate_weight: bfloat16 [2048, 5120], P('sp', 'tp'), may hold values from -0.125 to 0.125
- mixer_up_weight: bfloat16 [2048, 5120], P('sp', 'tp'), may hold values from -0.125 to 0.125
- mixer_down_weight: bfloat16 [5120, 2048], P('tp', 'sp'), may hold values from -0.078125 to 0.078125
Outputs:
- updated: bfloat16 [6144, 2048], P('sp', 'tp')
All inputs are finite; a program needn't handle non-finite values.
Results may differ from a plain program's by a relative error of at most 0.014.
Values may be sent and summed in bfloat16 or wider, within the bound.
A program may use at most 128 MiB of HBM per device.

v0:
```python
import jax
import jax.numpy as jnp
from jax import lax
from jax.sharding import PartitionSpec as P

DQK = 128
DV = 256


HIGHEST = lax.Precision.HIGHEST
EPSILON = 1e-06
LOWEST_LOG = -1e30


def carried_in(value, axis, join, neutral):
    count, mine = (lax.axis_size(axis), lax.axis_index(axis))
    pieces = jax.tree.map(lambda part: lax.all_gather(part, axis), value)
    subtotal = jax.tree.map(
        lambda part, zero: jnp.full_like(part, 0) + jnp.asarray(zero, part.dtype), value, neutral
    )

    def turn(position, subtotal):
        longer = join(subtotal, jax.tree.map(lambda part: part[position], pieces))
        return jax.tree.map(lambda new, old: jnp.where(position < mine, new, old), longer, subtotal)

    return lax.fori_loop(0, count - 1, turn, subtotal)


def heads_first(array, heads, width):
    return array.reshape(array.shape[0], heads, width).transpose(1, 0, 2)


def read_out(
    query_low, key_low, value_low, in_logs, running_log_total, memory, normalizer, stabilizer
):
    length = query_low.shape[1]
    causal = lax.broadcasted_iota(jnp.int32, (length, length), 0) >= lax.broadcasted_iota(
        jnp.int32, (length, length), 1
    )
    spread = running_log_total[:, :, None] - running_log_total[:, None, :] + in_logs[:, None, :]
    spread = jnp.where(causal[None], spread, -jnp.inf)
    carried = running_log_total + stabilizer[:, None]
    running = jnp.maximum(carried, jnp.max(spread, axis=-1))
    scores = jnp.einsum(
        "htd,hsd->hts", query_low, key_low, preferred_element_type=jnp.float32
    ) * DQK ** (-0.5)
    weights = jnp.exp(spread - running[:, :, None]) * scores
    scaled = jnp.exp(carried - running)
    scaled_query = query_low.astype(jnp.float32) * DQK ** (-0.5)
    numerator = jnp.einsum(
        "hts,hsv->htv", weights.astype(jnp.bfloat16), value_low, preferred_element_type=jnp.float32
    )
    numerator = numerator + scaled[:, :, None] * jnp.einsum(
        "hvd,htd->htv", memory, scaled_query, precision=HIGHEST
    )
    denominator = jnp.sum(weights, axis=-1) + scaled * jnp.einsum(
        "hd,htd->ht", normalizer, scaled_query, precision=HIGHEST
    )
    return numerator / jnp.maximum(jnp.abs(denominator), jnp.exp(-running))[:, :, None]


def fold_state(keyed, valued, in_logs, running_log_total, memory, normalizer, stabilizer):
    last = running_log_total[:, -1]
    lifted = last[:, None] - running_log_total + in_logs
    new_max = jnp.maximum(last + stabilizer, jnp.max(lifted, axis=-1))
    weights = jnp.exp(lifted - new_max[:, None])
    retained = jnp.exp(last + stabilizer - new_max)
    memory = retained[:, None, None] * memory + jnp.einsum(
        "hsv,hsd->hvd", weights[:, :, None] * valued, keyed, precision=HIGHEST
    )
    normalizer = retained[:, None] * normalizer + jnp.einsum(
        "hs,hsd->hd", weights, keyed, precision=HIGHEST
    )
    return (memory, normalizer, new_max)


def join_states(earlier, later):
    early_decay, early_memory, early_normalizer, early_max = earlier
    late_decay, late_memory, late_normalizer, late_max = later
    joined_max = jnp.maximum(late_decay + early_max, late_max)
    first_scale = jnp.exp(late_decay + early_max - joined_max)
    second_scale = jnp.exp(late_max - joined_max)
    memory = first_scale[:, None, None] * early_memory + second_scale[:, None, None] * late_memory
    normalizer = first_scale[:, None] * early_normalizer + second_scale[:, None] * late_normalizer
    return (early_decay + late_decay, memory, normalizer, joined_max)


def body(
    residual,
    query_matrix,
    key_matrix,
    value_matrix,
    output_gate_logit,
    input_gate_log,
    forget_gate_logit,
    extra_head_decay,
    head_norm_gain,
    projection,
    cell_output_gain,
    mixer_input_gain,
    mixer_gate_weight,
    mixer_up_weight,
    mixer_down_weight,
):
    tok_rows = residual.shape[0]
    width = residual.shape[1]
    heads_here = input_gate_log.shape[1]
    query_low = heads_first(query_matrix, heads_here, DQK)
    key_low = heads_first(key_matrix, heads_here, DQK)
    value_low = heads_first(value_matrix, heads_here, DV)
    keyed = key_low.astype(jnp.float32)
    valued = value_low.astype(jnp.float32)
    in_logs = input_gate_log.T
    running_log_total = jnp.cumsum(
        (jax.nn.log_sigmoid(forget_gate_logit) + extra_head_decay).T, axis=-1
    )
    zero_memory = jnp.zeros((heads_here, DV, DQK), jnp.float32)
    zero_normalizer = jnp.zeros((heads_here, DQK), jnp.float32)
    lowest = jnp.full((heads_here,), LOWEST_LOG, jnp.float32)
    local_memory, local_normalizer, local_max = fold_state(
        keyed, valued, in_logs, running_log_total, zero_memory, zero_normalizer, lowest
    )
    prior_decay, prior_memory, prior_normalizer, prior_max = carried_in(
        (running_log_total[:, -1], local_memory, local_normalizer, local_max),
        "sp",
        join_states,
        (jnp.zeros_like(lowest), zero_memory, zero_normalizer, lowest),
    )
    start_max = jnp.maximum(prior_decay, prior_max)
    lift = jnp.exp(prior_max - start_max)
    cells = read_out(
        query_low,
        key_low,
        value_low,
        in_logs,
        running_log_total,
        lift[:, None, None] * prior_memory,
        lift[:, None] * prior_normalizer,
        start_max,
    )
    centered = cells - jnp.mean(cells, axis=-1, keepdims=True)
    normed = centered * lax.rsqrt(jnp.mean(centered * centered, axis=-1, keepdims=True) + EPSILON)
    normed = normed * head_norm_gain.reshape(heads_here, DV)[:, None, :]
    normed = normed.transpose(1, 0, 2).reshape(tok_rows, heads_here * DV)
    gated = (normed * jax.nn.sigmoid(output_gate_logit.astype(jnp.float32))).astype(jnp.bfloat16)
    cols_here = width // lax.axis_size("tp")
    offset = lax.axis_index("tp") * cols_here
    columns = projection
    mixed = (
        lax.psum_scatter(
            lax.dot_general(
                columns, gated, (((0,), (1,)), ((), ())), preferred_element_type=jnp.float32
            ).astype(jnp.bfloat16),
            "tp",
            scatter_dimension=0,
            tiled=True,
        )
        .astype(jnp.float32)
        .T
    )
    squares = lax.psum(jnp.sum(mixed * mixed, axis=-1), "tp")
    mixed = (
        mixed
        * lax.rsqrt(squares / width + EPSILON)[:, None]
        * lax.dynamic_slice_in_dim(cell_output_gain, offset, cols_here, 0)
    )
    own_residual = lax.dynamic_slice_in_dim(residual, offset, cols_here, 1).astype(jnp.float32)
    first_sum = (own_residual + mixed).astype(jnp.bfloat16)
    own_first = lax.optimization_barrier(first_sum).astype(jnp.float32)
    first_total = lax.psum(jnp.sum(own_first * own_first, axis=-1), "tp")
    own_gain = lax.dynamic_slice_in_dim(mixer_input_gain, offset, cols_here, 0)
    normed_own = (own_first * lax.rsqrt(first_total / width + EPSILON)[:, None] * own_gain).astype(
        jnp.bfloat16
    )
    normed_rows = lax.all_gather(normed_own, "tp", axis=1, tiled=True)
    columns = normed_rows
    gate_value = jnp.dot(
        columns,
        lax.all_gather(mixer_gate_weight, "sp", axis=0, tiled=True),
        preferred_element_type=jnp.float32,
    )
    up_value = jnp.dot(
        columns,
        lax.all_gather(mixer_up_weight, "sp", axis=0, tiled=True),
        preferred_element_type=jnp.float32,
    )
    activated = (jax.nn.silu(gate_value) * up_value).astype(jnp.bfloat16)
    down_terms = jnp.dot(
        activated,
        lax.all_gather(mixer_down_weight, "sp", axis=1, tiled=True),
        preferred_element_type=jnp.float32,
    )
    channel_out = lax.psum_scatter(
        down_terms.astype(jnp.bfloat16), "tp", scatter_dimension=1, tiled=True
    ).astype(jnp.float32)
    return (own_first + 0.5 * channel_out).astype(jnp.bfloat16)


def solution(mesh):
    return jax.shard_map(
        body,
        mesh=mesh,
        in_specs=(
            P("sp", None),
            P("sp", "tp"),
            P("sp", "tp"),
            P("sp", "tp"),
            P("sp", "tp"),
            P("sp", "tp"),
            P("sp", "tp"),
            P("sp", "tp"),
            P("tp"),
            P("tp", None),
            P(),
            P(),
            P("sp", "tp"),
            P("sp", "tp"),
            P("tp", "sp"),
        ),
        out_specs=P("sp", "tp"),
        check_vma=False,
    )
```

profile of v0, /device:TPU:25, one launch (start us, length us, event | category | flops | bytes accessed | tf_op | source)
XLA Modules:
  0.0 487.9 jit_solution(3324282672585852311)
XLA Ops:
  6.6 0.9 fusion.53
  7.5 0.6 reduce-window.6
  8.7 0.9 fusion.71
  9.9 1.4 copy.54
  11.4 2.8 fusion.32
  14.4 0.6 dynamic-slice
  15.8 13.0 %all-gather.3 = f32[8,1,2]{2,1,0:T(1,128)S(1)} all-gather(f32[1,1,2]{2,1,0:T(1,128)S(1)} %fusion.59), channel_id=1, replica_groups=mesh['sp'=8,'tp'=4] {'sp'}, dimensions={0}, use_global_device_ids=true | all-gather | bytes 72 | tf_op jit(solution)/shard_map/all_gather | solution.py:17
  28.8 14.5 %all-reduce = f32[16]{0:T(128)S(1)} all-reduce(f32[16]{0:T(128)S(1)} %dynamic-update-slice), channel_id=2, replica_groups=mesh['sp'=8,'tp'=4] {'sp'}, use_global_device_ids=true, to_apply=%add | all-reduce | flops 16 | bytes 128
  43.4 0.3 fusion.40
  43.8 14.3 %all-gather.4 = f32[8,2,128]{2,1,0:T(2,128)S(1)} all-gather(f32[1,2,128]{2,1,0:T(2,128)S(1)} %add_bitcast_fusion.1), channel_id=4, replica_groups=mesh['sp'=8,'tp'=4] {'sp'}, dimensions={0}, use_global_device_ids=true | all-gather | bytes 9216 | tf_op jit(solution)/shard_map/all_gather | solution.py:17
  58.3 0.9 fusion.7
  59.3 3.4 all-gather.19.cloned.1.call-done
  62.7 8.3 %while.20 = (s32[]{:T(128)}, f32[2]{0:T(128)S(1)}, f32[2,256,128]{2,1,0:T(8,128)S(1)}, f32[2,128]{1,0:T(2,128)S(1)}, f32[2]{0:T(128)S(1)}, /*index=5*/s32[]{:T(1...) while((s32[]{:T(128)}, f32[2]{0:T(128)S(1)}, ...), condition=%wide.region_4.5_spmd.clone, body=%wide.region_3.4_spmd.clone.sunk | while | flops 328984 | bytes 789781 | solution.py:26
  62.7 1.1 fusion.90
  63.9 1.1 fusion.90
  65.1 1.1 fusion.90
  66.3 1.1 fusion.90
  67.5 1.1 fusion.90
  68.7 1.1 fusion.90
  69.8 1.1 fusion.90
  71.1 3.0 fusion.10
  74.1 0.7 fusion.36
  74.8 1.5 fusion.37
  76.4 2.4 fusion.69
  78.8 0.3 multiply_reduce_fusion
  79.2 1.5 fusion.28
  80.7 3.1 copy.47
  83.8 4.9 %fusion.9 = bf16[2048,768]{0,1:T(8,128)(2,1)} fusion(bf16[512,2048]{1,0:T(8,128)(2,1)S(1)} %copy-done, f32[768,512]{1,0:T(8,128)} %copy.47, bf16[768,512]{1,0:T(8,128)(2,1)S(1)} %copy-done.7), kind=kOutput, calls=%fused_computation.24 | convolution fusion | flops 1614544896 | bytes 7602176 | tf_op jit(solution)/shard_map/dot_general | solution.py:151
  88.8 0.7 all-gather.13.cloned.1.call-update
  89.5 0.8 dynamic_slice.38
  90.3 0.8 dynamic_slice.39
  91.0 44.6 %reduce-scatter.3.cloned.1.call-done = bf16[512,768]{0,1:T(8,128)(2,1)} async-done(((bf16[2048,768]{0,1:T(8,128)(2,1)}), bf16[512,768]{0,1:T(8,128)(2,1)}) %reduce-scatter.3.cloned.1.call-update) | async-done | bytes 786448 | tf_op jit(solution)/shard_map/reduce_scatter | solution.py:150
  135.7 1.4 fusion.15
  137.0 5.9 %psum.14 = f32[768]{0:T(1024)S(1)} all-reduce(f32[768]{0:T(1024)S(1)} %fusion.15), channel_id=1, replica_groups=mesh['sp'=8,'tp'=4] {'tp'}, use_global_device_ids=true, to_apply=%region_11.12 | all-reduce | flops 768 | bytes 6144 | tf_op jit(solution)/shard_map/psum | solution.py:161
  142.9 1.7 fusion.19
  144.8 6.0 %psum.15 = f32[768]{0:T(1024)S(1)} all-reduce(f32[768]{0:T(1024)S(1)} %fusion.20), channel_id=1, replica_groups=mesh['sp'=8,'tp'=4] {'tp'}, use_global_device_ids=true, to_apply=%region_13.14 | all-reduce | flops 768 | bytes 6144 | tf_op jit(solution)/shard_map/psum | solution.py:170
  150.8 1.1 fusion.22
  152.0 0.5 all-gather.15.cloned.1.call-update
  152.6 0.5 all-gather.17.cloned.1.call-update
  153.1 0.3 reduce-scatter.5.cloned.1.call-start
  153.4 68.8 %all-gather.13.cloned.1.call-done = bf16[2048,1280]{1,0:T(8,128)(2,1)} async-done(((bf16[256,1280]{1,0:T(8,128)(2,1)}), bf16[2048,1280]{1,0:T(8,128)(2,1)}) %all-gather.13.cloned.1.call-update) | async-done | bytes 5242896 | tf_op jit(solution)/shard_map/all_gather | solution.py:179
  222.2 30.3 %all-gather.11.cloned.1.call-done = bf16[768,2048]{1,0:T(8,128)(2,1)} async-done(((bf16[768,512]{1,0:T(8,128)(2,1)}), bf16[768,2048]{1,0:T(8,128)(2,1)}) %all-gather.11.cloned.1.call-update) | async-done | bytes 3145744 | tf_op jit(solution)/shard_map/all_gather | solution.py:175
  252.5 9.6 %fusion.72 = f32[768,1280]{1,0:T(8,128)} fusion(bf16[768,2048]{1,0:T(8,128)(2,1)} %all-gather.11.cloned.1.call-done, bf16[2048,1280]{1,0:T(8,128)(2,1)} %all-gather.13.cloned.1.call-done), kind=kOutput, calls=%fused_computation.118 | convolution fusion | flops 4026531840 | bytes 12320768 | tf_op jit(solution)/shard_map/dot_general | solution.py:177
  262.0 76.2 %all-gather.15.cloned.1.call-done = bf16[2048,1280]{1,0:T(8,128)(2,1)} async-done(((bf16[256,1280]{1,0:T(8,128)(2,1)}), bf16[2048,1280]{1,0:T(8,128)(2,1)}) %all-gather.15.cloned.1.call-update) | async-done | bytes 5242896 | tf_op jit(solution)/shard_map/all_gather | solution.py:184
  338.3 86.8 %all-gather.17.cloned.1.call-done = bf16[1280,2048]{1,0:T(8,128)(2,1)} async-done(((bf16[1280,256]{1,0:T(8,128)(2,1)}), bf16[1280,2048]{1,0:T(8,128)(2,1)}) %all-gather.17.cloned.1.call-update) | async-done | bytes 5242896 | tf_op jit(solution)/shard_map/all_gather | solution.py:190
  425.1 16.0 %convolution_convert_fusion.1 = bf16[768,2048]{1,0:T(8,128)(2,1)} fusion(bf16[1280,2048]{1,0:T(8,128)(2,1)} %all-gather.17.cloned.1.call-done, bf16[768,2048]{1,0:T(8,128)(2,1)} %all-gather.11.cloned.1.call-done, bf16[2048,1280]{1,0:T(8,128)(2,1)} %all-gather.15.cloned.1.call-done, f32[768,1280]{1,0:T(8,128)} %fusion.72), kind=kOutput, calls=%fused_computation.23 | convolution fusion | flops 8060534784 | bytes 20709376 | tf_op jit(solution)/shard_map/dot_general | solution.py:188
  441.1 37.7 %reduce-scatter.5.cloned.1.call-done = bf16[768,512]{1,0:T(8,128)(2,1)} async-done(((bf16[768,2048]{1,0:T(8,128)(2,1)}), bf16[768,512]{1,0:T(8,128)(2,1)}) %reduce-scatter.5.cloned.1.call-update) | async-done | bytes 786448 | tf_op jit(solution)/shard_map/reduce_scatter | solution.py:193
  478.8 2.2 fusion.23
  (80 shorter events, 3.3 us)
Async XLA Ops:
  6.5 77.3 %copy-start = (bf16[512,2048]{1,0:T(8,128)(2,1)S(1)}, bf16[512,2048]{1,0:T(8,128)(2,1)}, u32[]{:S(2)}) copy-start(bf16[512,2048]{1,0:T(8,128)(2,1)} %param.26) | copy-start | bytes 6291460
  6.5 7.8 %copy-start.8 = (u32[32]{0:T(128)S(1)}, u32[32]{0:T(128)}, u32[]{:S(2)}) copy-start(u32[32]{0:T(128)} %constant.77) | copy-start | bytes 388
  6.5 36.9 %copy-start.4 = (bf16[768,256]{1,0:T(8,128)(2,1)S(1)}, bf16[768,256]{1,0:T(8,128)(2,1)}, u32[]{:S(2)}) copy-start(bf16[768,256]{1,0:T(8,128)(2,1)} %param.19) | copy-start | bytes 1179652
  6.5 36.8 %copy-start.6 = (f32[512]{0:T(512)S(1)}, f32[512]{0:T(512)}, u32[]{:S(2)}) copy-start(f32[512]{0:T(512)} %param.25) | copy-start | bytes 6148
  6.5 56.1 %all-gather.19.cloned.1.call-start = ((), (), s32[]{:S(2)}) async-start(), calls=%async_computation.8 | async-start | bytes 2359296 | tf_op jit(solution)/shard_map/all_gather | solution.py:17
  7.5 50.8 %copy-start.5 = (f32[768,2]{0,1:T(2,128)S(1)}, f32[768,2]{0,1:T(2,128)}, u32[]{:S(2)}) copy-start(f32[768,2]{0,1:T(2,128)} %param.22) | copy-start | bytes 18436
  11.3 17.4 %copy-start.1 = (bf16[768,512]{0,1:T(8,128)(2,1)}, bf16[768,512]{0,1:T(8,128)(2,1)S(1)}, u32[]{:S(2)}) copy-start(bf16[768,512]{0,1:T(8,128)(2,1)S(1)} %copy.54) | copy-start | bytes 2359300
  14.3 121.4 %reduce-scatter.3.cloned.1.call-start = ((), (), s32[]{:S(2)}) async-start(), calls=%async_computation.2 | async-start | bytes 3932160 | tf_op jit(solution)/shard_map/reduce_scatter | solution.py:150
  58.3 12.8 %copy-start.3 = (bf16[768,256]{1,0:T(8,128)(2,1)S(1)}, bf16[768,256]{1,0:T(8,128)(2,1)}, u32[]{:S(2)}) copy-start(bf16[768,256]{1,0:T(8,128)(2,1)} %param.18) | copy-start | bytes 1179652
  74.0 2.4 copy-start.2
  80.7 3.1 copy-start.7
  88.7 133.4 %all-gather.13.cloned.1.call-start = ((), (), s32[]{:S(2)}) async-start(), calls=%async_computation.4 | async-start | bytes 5898240 | tf_op jit(solution)/shard_map/all_gather | solution.py:179
  89.5 163.0 %all-gather.11.cloned.1.call-start = ((), (), s32[]{:S(2)}) async-start(), calls=%async_computation.3 | async-start | bytes 3932160 | tf_op jit(solution)/shard_map/all_gather | solution.py:175
  152.0 186.3 %all-gather.15.cloned.1.call-start = ((), (), s32[]{:S(2)}) async-start(), calls=%async_computation.5 | async-start | bytes 5898240 | tf_op jit(solution)/shard_map/all_gather | solution.py:184
  152.6 272.5 %all-gather.17.cloned.1.call-start = ((), (), s32[]{:S(2)}) async-start(), calls=%async_computation.6 | async-start | bytes 5898240 | tf_op jit(solution)/shard_map/all_gather | solution.py:190
  153.1 325.6 %reduce-scatter.5.cloned.1.call-start = ((), (), s32[]{:S(2)}) async-start(), calls=%async_computation.7 | async-start | bytes 3932160 | tf_op jit(solution)/shard_map/reduce_scatter | solution.py:193
Sparse Core Ops, SparseCore 0:
  14.4 48.2 all-gather.18
  88.8 46.7 reduce-scatter.2
  137.9 84.2 all-gather.12
  223.6 28.8 all-gather.10
  254.5 83.6 all-gather.14
  340.1 84.8 all-gather.16
  441.2 37.5 reduce-scatter.4
where the time goes:
time: 491 us; the launch traced here: 488 us
  waiting for transfers between devices  350 us (71%)
  blocking collectives  53.6 us (11%)
  matrix products  41 us (8%)
  other arithmetic  21.3 us (4%)
  between operations  14.3 us (3%)
  local copies, waits for them, and re-layouts  7.45 us (2%)
    all_gather x1, waiting for transfers between devices, body(): lax.all_gather(mixer_down_weight, 'sp', axis=1, tiled=True)  86.8 us
    all_gather x1, waiting for transfers between devices, body(): lax.all_gather(mixer_up_weight, 'sp', axis=0, tiled=True)  76.2 us
    all_gather x1, waiting for transfers between devices, body(): lax.all_gather(mixer_gate_weight, 'sp', axis=0, tiled=True)  68.8 us
    reduce_scatter x1, waiting for transfers between devices, body(): lax.psum_scatter(lax.dot_general(columns, gated, (((0,), (1,)), ((), ()))...  44.6 us
    reduce_scatter x1, waiting for transfers between devices, body(): lax.psum_scatter(down_terms.astype(jnp.bfloat16), 'tp', scatter_dimension...  37.7 us
    all_gather x1, waiting for transfers between devices, body(): normed_rows = lax.all_gather(normed_own, 'tp', axis=1, tiled=True)  30.3 us
    all_gather x2, blocking collectives, carried_in(): pieces = jax.tree.map(lambda part: lax.all_gather(part, axis), value)  27.3 us
    dot_general x1, matrix products, body(): jnp.dot(activated, lax.all_gather(mixer_down_weight, 'sp', axis=1, tiled=...  16 us
  transfers between devices with their start and end apart: 7, of which 7 were waited for; matrix products, arithmetic and copies ran while one was open for 4% of the time, Pallas kernels for 0%

commit v1 on v0

v1 whole, which is shorter than its diff:
```python
import functools

import jax
import jax.numpy as jnp
from jax import lax
from jax.experimental import pallas as pl
from jax.experimental.pallas import tpu as pltpu
from jax.sharding import PartitionSpec as P

DQK = 128
DV = 256
MESH = pl.DeviceIdType.MESH
VMEM = pl.BlockSpec(memory_space=pltpu.VMEM)
ANY = pl.BlockSpec(memory_space=pl.ANY)
VMEM_BYTES = 62 * 1024 * 1024

HIGHEST = lax.Precision.HIGHEST
EPSILON = 1e-06
LOWEST_LOG = -1e30


def heads_first(array, heads, width):
    return array.reshape(array.shape[0], heads, width).transpose(1, 0, 2)


def fold_state(keyed, valued, in_logs, running_log_total, memory, normalizer, stabilizer):
    last = running_log_total[:, -1]
    lifted = last[:, None] - running_log_total + in_logs
    new_max = jnp.maximum(last + stabilizer, jnp.max(lifted, axis=-1))
    weights = jnp.exp(lifted - new_max[:, None])
    retained = jnp.exp(last + stabilizer - new_max)
    memory = retained[:, None, None] * memory + jnp.einsum(
        "hsv,hsd->hvd", weights[:, :, None] * valued, keyed, precision=HIGHEST
    )
    normalizer = retained[:, None] * normalizer + jnp.einsum(
        "hs,hsd->hd", weights, keyed, precision=HIGHEST
    )
    return (memory, normalizer, new_max)


def copy_to(source, target, sems, slot, peer):
    return pltpu.make_async_remote_copy(
        source, target, sems.at[(0, *slot)], sems.at[(1, *slot)], device_id=peer, device_id_type=MESH
    )


def layer_kernel(
    ranks, count, heads, carried_by_hand, memory_ref, aux_ref, cum_row, in_row, cum_col, query_ref,
    key_ref, value_ref, ogate_ref, head_gain, residual_ref, out_gain, in_gain, projection_ref,
    gate_ref, up_ref, down_ref, out_ref, slots, aux_slots, memory, aux, gate_w, up_w, down_w,
    weight, gated, blocks, normed, first, active, to_core, from_core, to_chip, from_chip,
    state_sems, aux_sems, line_sems, cross_sems, local_sems, proj_sems, gated_sems, sum_sems,
):
    sp, me = lax.axis_index("sp"), lax.axis_index("tp")
    row, col = sp // 2, lax.rem(sp, 2)
    depth = ranks // 2
    core = lax.rem(me, 2)
    mate = me + 1 - 2 * core
    chips = count // 2
    rows_all, width = residual_ref.shape
    cols = out_ref.shape[1]
    inner = value_ref.shape[1]
    pending = []

    barrier = pltpu.get_barrier_semaphore()
    for axis, size, at in (("sp", ranks, sp), ("tp", count, me)):
        for step in range(1, size):
            pl.semaphore_signal(
                barrier, inc=1, device_id={axis: lax.rem(at + step, size)}, device_id_type=MESH
            )
    pl.semaphore_wait(barrier, ranks + count - 2)

    def when(condition, action):
        pl.when(condition)(action)

    def state_copies(step):
        peer = {"sp": lax.rem(sp + step, ranks)}
        return (
            copy_to(memory_ref, slots.at[step - 1], state_sems, (step - 1,), peer),
            copy_to(aux_ref, aux_slots.at[step - 1], aux_sems, (step - 1,), peer),
        )

    for step in range(1, ranks):

        @pl.when(sp + step < ranks)
        def _():
            for copy in state_copies(step):
                copy.start()

    half = down_w.shape[1] // 2
    high = gate_ref.shape[0]

    def views(kind, owner):
        rows = pl.ds(pl.multiple_of(owner * high, high), high)
        if kind == 0:
            return gate_ref, gate_w.at[rows, :]
        if kind == 1:
            return up_ref, up_w.at[rows, :]
        rows = pl.ds(0 if kind == 2 else half, half)
        return down_ref.at[rows, :], down_w.at[owner, rows, :]

    other = 1 - col
    line_slot = lambda way: 1 if way > 0 else 0

    def along(kind, step, column, mine, way):
        owner = (row - step) * 2 + column
        source, target = views(kind, owner)
        if step != 0 or not mine:
            source = target
        slot = (kind, 0 if mine else 1, abs(step), line_slot(way))
        return copy_to(source, target, line_sems, slot, {"sp": sp + 2 * way})

    def across(kind, step):
        owner = (row - step) * 2 + col
        source, target = views(kind, owner)
        if step != 0:
            source = target
        slot = (kind, step + depth - 1)
        return copy_to(source, target, cross_sems, slot, {"sp": row * 2 + other})

    def crossed(kind, step):
        owner = (row - step) * 2 + other
        source, target = views(kind, owner)
        return copy_to(target, target, cross_sems, (kind, step + depth - 1), {"sp": row * 2 + other})

    def came(kind, step, column, mine):
        owner = (row - step) * 2 + column
        source, target = views(kind, owner)
        way = 1 if step > 0 else -1
        slot = (kind, 0 if mine else 1, abs(step) - 1, line_slot(way))
        return copy_to(target, target, line_sems, slot, {"sp": sp})

    def exists(way):
        return jnp.logical_and(row + way >= 0, row + way < depth)

    def send_along(kind, step, column, mine, way):
        def start():
            along(kind, step, column, mine, way).start()

        has = jnp.logical_and(row - step >= 0, row - step < depth)
        when(jnp.logical_and(has, exists(way)), start)
        pending.append((jnp.logical_and(has, exists(way)), along(kind, step, column, mine, way)))

    def send_across(kind, step):
        has = jnp.logical_and(row - step >= 0, row - step < depth)
        when(has, lambda: across(kind, step).start())
        pending.append((has, across(kind, step)))

    def stage(step, kinds):
        for kind in kinds:
            for column, mine in ((col, True), (other, False)):
                if kind < 3 and not mine:
                    continue
                for way in (1, -1):
                    has = jnp.logical_and(row - way * step >= 0, row - way * step < depth)
                    when(has, lambda: came(kind, way * step, column, mine).wait_recv())
                    if step < depth - 1:
                        send_along(kind, way * step, column, mine, way)
                    if kind < 3:
                        send_across(kind, way * step)

    def finish(kinds):
        for kind in kinds:
            steps = range(1 - depth, depth) if kind < 3 else ()
            for step in steps:
                has = jnp.logical_and(row - step >= 0, row - step < depth)
                when(has, lambda: crossed(kind, step).wait_recv())

    def own(kind):
        source, target = views(kind, sp)
        return pltpu.make_async_copy(source, target, local_sems.at[kind])

    def spread(source, whole, sems):
        sent = [copy_to(source, whole.at[me], sems, (0,), {"tp": mate})]
        for step in range(1, chips):
            peer = {"tp": lax.rem(me + 2 * step, count)}
            sent.append(copy_to(source, whole.at[me], sems, (2 * step,), peer))
        for copy in sent:
            copy.start()
        return sent

    def relay(whole, sems):
        sent = []
        for step in range(1, chips):
            owner = lax.rem(me - 2 * step + count, count)
            block = whole.at[owner]
            copy_to(block, block, sems, (2 * step,), {"tp": mate}).wait_recv()
            sent.append(copy_to(block, block, sems, (2 * step - 1,), {"tp": mate}))
            sent[-1].start()
        return sent

    def collect(whole, sems):
        for step in range(chips):
            owner = lax.rem(mate - 2 * step + count, count)
            block = whole.at[owner]
            slot = 0 if step == 0 else 2 * step - 1
            copy_to(block, block, sems, (slot,), {"tp": mate}).wait_recv()

    if carried_by_hand:
        for kind in range(4):
            if kind == 3:
                send_across(3, 0)
            for way in (1, -1):
                send_along(kind, 0, col, True, way)
            if kind < 3:
                send_across(kind, 0)
            own(kind).start()
    else:
        for ref, whole, at in ((gate_ref, gate_w, 0), (up_ref, up_w, 1)):
            pltpu.make_async_copy(ref, whole, local_sems.at[at]).start()
        pltpu.make_async_copy(down_ref, down_w.at[0], local_sems.at[2]).start()
    own_weight = pltpu.make_async_copy(projection_ref, weight.at[me], local_sems.at[4])
    own_weight.start()
    sent = spread(projection_ref, weight, proj_sems)

    memory[...] = jnp.zeros_like(memory)
    aux[...] = jnp.zeros_like(aux)
    aux[heads : 2 * heads, :] = jnp.full((heads, DQK), LOWEST_LOG, jnp.float32)
    for step in range(ranks - 1, 0, -1):

        @pl.when(sp >= step)
        def _():
            for copy in state_copies(step):
                copy.wait_recv()
            late = aux_slots[step - 1]
            for head in range(heads):
                rows = pl.ds(head * DV, DV)
                early_max = aux[heads + head : heads + head + 1, :]
                late_max = late[heads + head : heads + head + 1, :]
                late_decay = late[2 * heads + head : 2 * heads + head + 1, :]
                joined = jnp.maximum(late_decay + early_max, late_max)
                before = jnp.exp(late_decay + early_max - joined)
                after = jnp.exp(late_max - joined)
                memory[rows, :] = before * memory[rows, :] + after * slots[
                    step - 1, rows, :
                ].astype(jnp.float32)
                aux[head : head + 1, :] = (
                    before * aux[head : head + 1, :] + after * late[head : head + 1, :]
                )
                aux[heads + head : heads + head + 1, :] = joined
                aux[2 * heads + head : 2 * heads + head + 1, :] = (
                    aux[2 * heads + head : 2 * heads + head + 1, :] + late_decay
                )

    if carried_by_hand:
        crossed(3, 0).wait_recv()
        for way in (1, -1):
            send_along(3, 0, other, False, way)
        stage(1, (0,))

    tile = rows_all // 3
    for head in range(heads):
        prior_max = aux[heads + head : heads + head + 1, :]
        start_max = jnp.maximum(aux[2 * heads + head : 2 * heads + head + 1, :], prior_max)
        lift = jnp.exp(prior_max - start_max) * DQK ** (-0.5)
        memory[head * DV : (head + 1) * DV, :] = memory[head * DV : (head + 1) * DV, :] * lift
        aux[head : head + 1, :] = aux[head : head + 1, :] * lift
        aux[2 * heads + head : 2 * heads + head + 1, :] = start_max

    def read(at, unused):
        start = pl.multiple_of(at * tile, tile)
        rows = pl.ds(start, tile)
        causal = start + lax.broadcasted_iota(
            jnp.int32, (tile, rows_all), 0
        ) >= lax.broadcasted_iota(jnp.int32, (tile, rows_all), 1)
        for head in range(heads):
            keys = slice(head * DQK, (head + 1) * DQK)
            values = slice(head * DV, (head + 1) * DV)
            query = query_ref[rows, keys]
            total = cum_col[rows, head : head + 1]
            spread_log = total - cum_row[head : head + 1, :] + in_row[head : head + 1, :]
            spread_log = jnp.where(causal, spread_log, -jnp.inf)
            carried = total + aux[2 * heads + head : 2 * heads + head + 1, :1]
            running = jnp.maximum(carried, jnp.max(spread_log, axis=-1, keepdims=True))
            scores = lax.dot_general(
                query, key_ref[:, keys], (((1,), (1,)), ((), ())),
                preferred_element_type=jnp.float32,
            ) * DQK ** (-0.5)
            weights = jnp.exp(spread_log - running) * scores
            scaled = jnp.exp(carried - running)
            wide = query.astype(jnp.float32)
            numerator = jnp.dot(
                weights.astype(jnp.bfloat16), value_ref[:, values],
                preferred_element_type=jnp.float32,
            ) + scaled * lax.dot_general(
                wide, memory[values, :], (((1,), (1,)), ((), ())), precision=HIGHEST,
                preferred_element_type=jnp.float32,
            )
            denominator = jnp.sum(weights, axis=-1, keepdims=True) + scaled * jnp.sum(
                wide * aux[head : head + 1, :], axis=-1, keepdims=True
            )
            cell = numerator / jnp.maximum(jnp.abs(denominator), jnp.exp(-running))
            centered = cell - jnp.mean(cell, axis=-1, keepdims=True)
            cell = centered * lax.rsqrt(
                jnp.mean(centered * centered, axis=-1, keepdims=True) + EPSILON
            )
            cell = cell * head_gain[:, values]
            gate = ogate_ref[rows, values].astype(jnp.float32)
            gated[rows, values] = (cell * jax.nn.sigmoid(gate)).astype(jnp.bfloat16)
        return unused

    lax.fori_loop(0, 3, read, 0)
    sent += spread(gated, blocks, gated_sems)
    blocks[me] = gated[...]
    if carried_by_hand:
        stage(1, (1, 2, 3))
    sent += relay(weight, proj_sems)
    if carried_by_hand:
        stage(2, (0, 1))
    sent += relay(blocks, gated_sems)
    collect(weight, proj_sems)
    own_weight.wait()
    collect(blocks, gated_sems)

    def turn(at, unused):
        rows = pl.ds(pl.multiple_of(at * tile, tile), tile)
        mixed = jnp.zeros((tile, width), jnp.float32)
        for block in range(count):
            mixed = mixed + jnp.dot(
                blocks[block, rows, :], weight[block], preferred_element_type=jnp.float32
            )
        scale = lax.rsqrt(jnp.mean(mixed * mixed, axis=-1, keepdims=True) + EPSILON)
        total = residual_ref[rows, :].astype(jnp.float32) + mixed * scale * out_gain[...]
        total = total.astype(jnp.bfloat16)
        first[rows, :] = total
        wide = total.astype(jnp.float32)
        scale = lax.rsqrt(jnp.mean(wide * wide, axis=-1, keepdims=True) + EPSILON)
        normed[rows, :] = (wide * scale * in_gain[...]).astype(jnp.bfloat16)
        return unused

    lax.fori_loop(0, 3, turn, 0)

    if carried_by_hand:
        stage(2, (2, 3))
        stage(3, (0, 1))
        finish((0, 1))
        own(0).wait()
        own(1).wait()
    else:
        for ref, whole, at in ((gate_ref, gate_w, 0), (up_ref, up_w, 1)):
            pltpu.make_async_copy(ref, whole, local_sems.at[at]).wait()

    def mix(at, unused):
        rows = pl.ds(pl.multiple_of(at * tile, tile), tile)
        left = normed[rows, :]
        gate = jnp.dot(left, gate_w[...], preferred_element_type=jnp.float32)
        up = jnp.dot(left, up_w[...], preferred_element_type=jnp.float32)
        active[rows, :] = (gate / (1.0 + jnp.exp(-gate)) * up).astype(jnp.bfloat16)
        return unused

    if carried_by_hand:
        stage(3, (2, 3))
    lax.fori_loop(0, 3, mix, 0)
    if carried_by_hand:
        finish((2, 3))
        own(2).wait()
        own(3).wait()
    else:
        pltpu.make_async_copy(down_ref, down_w.at[0], local_sems.at[2]).wait()

    def term(target):
        if carried_by_hand:
            each = cols // down_w.shape[2]
            return jnp.concatenate(
                [
                    jnp.dot(active[...], down_w[target * each + at],
                            preferred_element_type=jnp.float32)
                    for at in range(each)
                ],
                axis=1,
            )
        start = pl.multiple_of(target * cols, cols)
        return jnp.dot(
            active[...], down_w[0, :, pl.ds(start, cols)], preferred_element_type=jnp.float32
        )

    def send(source, target, kind, at, peer):
        return copy_to(source.at[at], target.at[at], sum_sems.at[kind], (at,), {"tp": peer})

    copies = []
    for step in range(1, chips):
        away = lax.rem(me + 2 * step, count)
        to_core[step] = term(away + 1 - 2 * core).astype(jnp.bfloat16)
        hop = send(to_core, from_core, 0, step, mate)
        hop.start()
        mine = term(away)
        hop.wait_recv()
        to_chip[step] = (mine + from_core[step].astype(jnp.float32)).astype(jnp.bfloat16)
        far = send(to_chip, from_chip, 1, step, away)
        far.start()
        copies += [hop, far]
    to_core[0] = term(mate).astype(jnp.bfloat16)
    hop = send(to_core, from_core, 0, 0, mate)
    hop.start()
    result = term(me)
    hop.wait_recv()
    result = result + from_core[0].astype(jnp.float32)
    for far in copies[1::2]:
        far.wait_recv()
    for step in range(1, chips):
        result = result + from_chip[step].astype(jnp.float32)
    own_first = first[:, pl.ds(pl.multiple_of(me * cols, cols), cols)]
    out_ref[...] = (own_first.astype(jnp.float32) + 0.5 * result).astype(jnp.bfloat16)
    for copy in copies + [hop] + sent:
        copy.wait_send()
    for condition, copy in pending:
        when(condition, copy.wait_send)
    for step in range(1, ranks):

        @pl.when(sp + step < ranks)
        def _():
            for copy in state_copies(step):
                copy.wait_send()


def layer(states, logs, cell_inputs, residual, gains, weights):
    decay, memory, normalizer, maximum = states
    running_log_total, in_logs = logs
    ranks, count = lax.axis_size("sp"), lax.axis_size("tp")
    heads = decay.shape[0]
    rows, width = residual.shape
    projection, gate_weight, up_weight, down_weight = weights
    hidden = gate_weight.shape[1]
    inner = projection.shape[0]
    carried_by_hand = ranks == 8
    if carried_by_hand:
        down_shape = (ranks, hidden, down_weight.shape[1])
    else:
        gate_weight = lax.all_gather(gate_weight, "sp", axis=0, tiled=True)
        up_weight = lax.all_gather(up_weight, "sp", axis=0, tiled=True)
        down_weight = lax.all_gather(down_weight, "sp", axis=1, tiled=True)
        down_shape = (1, hidden, width)
    fill = lambda row: jnp.broadcast_to(row[:, None], (heads, DQK))
    aux = jnp.concatenate([normalizer, fill(maximum), fill(decay)])
    height = -(-3 * heads // 8) * 8
    aux = jnp.pad(aux, ((0, height - 3 * heads), (0, 0)))
    low = memory.reshape(heads * DV, DQK).astype(jnp.bfloat16)
    chips, cols, depth = count // 2, width // count, ranks // 2
    buffer = pltpu.VMEM((chips, rows, cols), jnp.bfloat16)
    dma = pltpu.SemaphoreType.DMA
    return pl.pallas_call(
        functools.partial(layer_kernel, ranks, count, heads, carried_by_hand),
        out_shape=jax.ShapeDtypeStruct((rows, cols), jnp.bfloat16),
        in_specs=[VMEM] * 13 + [ANY] * 4,
        out_specs=VMEM,
        scratch_shapes=[
            pltpu.VMEM((ranks - 1, heads * DV, DQK), jnp.bfloat16),
            pltpu.VMEM((ranks - 1, height, DQK), jnp.float32),
            pltpu.VMEM((heads * DV, DQK), jnp.float32),
            pltpu.VMEM((height, DQK), jnp.float32),
            pltpu.VMEM((width, hidden), jnp.bfloat16),
            pltpu.VMEM((width, hidden), jnp.bfloat16),
            pltpu.VMEM(down_shape, jnp.bfloat16),
            pltpu.VMEM((count, inner, width), jnp.bfloat16),
            pltpu.VMEM((rows, inner), jnp.bfloat16),
            pltpu.VMEM((count, rows, inner), jnp.bfloat16),
            pltpu.VMEM((rows, width), jnp.bfloat16),
            pltpu.VMEM((rows, width), jnp.bfloat16),
            pltpu.VMEM((rows, hidden), jnp.bfloat16),
            buffer, buffer, buffer, buffer,
            dma((2, ranks - 1)),
            dma((2, ranks - 1)),
            dma((2, 4, 2, depth, 2)),
            dma((2, 4, 2 * depth - 1)),
            dma((5,)),
            dma((2, count)),
            dma((2, count)),
            dma((2, 2, chips)),
        ],
        compiler_params=pltpu.CompilerParams(
            collective_id=0, has_side_effects=True, vmem_limit_bytes=VMEM_BYTES
        ),
        name="layer",
    )(
        low, aux, running_log_total, in_logs, running_log_total.T, *cell_inputs, residual,
        *gains, projection, gate_weight, up_weight, down_weight,
    )


def body(
    residual,
    query_matrix,
    key_matrix,
    value_matrix,
    output_gate_logit,
    input_gate_log,
    forget_gate_logit,
    extra_head_decay,
    head_norm_gain,
    projection,
    cell_output_gain,
    mixer_input_gain,
    mixer_gate_weight,
    mixer_up_weight,
    mixer_down_weight,
):
    heads_here = input_gate_log.shape[1]
    key_low = heads_first(key_matrix, heads_here, DQK)
    value_low = heads_first(value_matrix, heads_here, DV)
    keyed = key_low.astype(jnp.float32)
    valued = value_low.astype(jnp.float32)
    in_logs = input_gate_log.T
    running_log_total = jnp.cumsum(
        (jax.nn.log_sigmoid(forget_gate_logit) + extra_head_decay).T, axis=-1
    )
    zero_memory = jnp.zeros((heads_here, DV, DQK), jnp.float32)
    zero_normalizer = jnp.zeros((heads_here, DQK), jnp.float32)
    lowest = jnp.full((heads_here,), LOWEST_LOG, jnp.float32)
    local_memory, local_normalizer, local_max = fold_state(
        keyed, valued, in_logs, running_log_total, zero_memory, zero_normalizer, lowest
    )
    return layer(
        (running_log_total[:, -1], local_memory, local_normalizer, local_max),
        (running_log_total, in_logs),
        (query_matrix, key_matrix, value_matrix, output_gate_logit, head_norm_gain[None]),
        residual,
        (cell_output_gain[None], mixer_input_gain[None]),
        (projection, mixer_gate_weight, mixer_up_weight, mixer_down_weight),
    )


def solution(mesh):
    return jax.shard_map(
        body,
        mesh=mesh,
        in_specs=(
            P("sp", None),
            P("sp", "tp"),
            P("sp", "tp"),
            P("sp", "tp"),
            P("sp", "tp"),
            P("sp", "tp"),
            P("sp", "tp"),
            P("sp", "tp"),
            P("tp"),
            P("tp", None),
            P(),
            P(),
            P("sp", "tp"),
            P("sp", "tp"),
            P("tp", "sp"),
        ),
        out_specs=P("sp", "tp"),
        check_vma=False,
    )
```

time: 491 us -> 216 us (0.44)
  waiting for transfers between devices: 350 us -> 0 us
  Pallas kernels: 0 us -> 206 us
  blocking collectives: 53.6 us -> 0 us
  matrix products: 41 us -> 1.8 us
  other arithmetic: 21.3 us -> 1.94 us
  between operations: 14.3 us -> 0.09 us
    all_gather x5 -> x0, waiting for transfers between devices: 266 us -> none  [the longest x1 86.8 us: body(): lax.all_gather(mixer_down_weight, 'sp', axis=1, tiled=True)]
    pallas_call x0 -> x1, Pallas kernels: none -> 206 us  [layer(): pl.pallas_call(functools.partial(layer_kernel, ranks, count, heads, carri...]
    reduce_scatter x2 -> x0, waiting for transfers between devices: 82.3 us -> none  [the longest x1 44.6 us: body(): lax.psum_scatter(lax.dot_general(columns, gated, (((0,), (1,)), ((), ()))...]
    dot_general x7 -> x0, matrix products: 37.9 us -> none  [the longest x1 16 us: body(): jnp.dot(activated, lax.all_gather(mixer_down_weight, 'sp', axis=1, tiled=...]
    all_gather x2 -> x0, blocking collectives: 27.3 us -> none  [carried_in(): pieces = jax.tree.map(lambda part: lax.all_gather(part, axis), value)]
    unnamed x1 -> x0, blocking collectives: 14.5 us -> none
    psum x2 -> x0, blocking collectives: 11.8 us -> none  [the longest x1 5.95 us: body(): first_total = lax.psum(jnp.sum(own_first * own_first, axis=-1), 'tp')]
    select_n x21 -> x0, other arithmetic: 8.15 us -> none  [turn(): jnp.where(position < mine, new, old)]
  transfers between devices with their start and end apart: 7 -> 0, of which waited for: 7 -> 0; matrix products, arithmetic and copies ran while one was open for 4% -> 0% of each run, Pallas kernels for 0% -> 0%
where the time goes in v1:
time: 216 us
  Pallas kernels  206 us (95%)
  local copies, waits for them, and re-layouts  6.18 us (3%)
    pallas_call x1, Pallas kernels, layer(): pl.pallas_call(functools.partial(layer_kernel, ranks, count, heads, carri...  206 us

profile of v1, /device:TPU:25, one launch (start us, length us, event | category | flops | bytes accessed | tf_op | source)
XLA Modules:
  0.0 215.7 jit_solution(10641095510582364061)
XLA Ops:
  0.0 0.7 fusion.15
  0.8 0.6 reduce-window.6
  1.3 0.2 slice_reduce_fusion
  1.5 0.2 reduce-window.9
  1.7 0.1 broadcast_add_fusion
  1.8 0.2 copy.23
  1.9 0.0 copy-start
  2.0 0.1 pad.7.clone
  2.0 0.7 copy.28.cum_row
  2.8 0.0 copy-start.1
  2.8 0.9 copy.24
  3.7 0.1 fusion.12
  3.8 0.0 copy-start.2
  3.9 0.1 pad.6.clone
  3.9 0.7 copy.29.in_row
  4.7 0.1 subtract_exponential_fusion
  4.8 0.0 copy-done
  4.8 0.1 copy.30
  4.9 0.0 copy-done.1
  4.9 0.3 fusion.9
  5.2 0.1 broadcast_add_fusion.1
  5.3 0.1 maximum_maximum_fusion
  5.3 0.6 pad.4.aux_ref
  6.0 0.1 copy.25
  6.1 0.0 copy-done.2
  6.1 0.3 copy.32
  6.4 1.5 fusion.5
  7.9 205.7 %layer.1 = bf16[768,512]{1,0:T(8,128)(2,1)} custom-call(bf16[512,128]{1,0:T(8,128)(2,1)} %bitcast.59, f32[8,128]{1,0:T(8,128)} %pad.4.aux_ref, f32[2,768]{1,0:T(2,128)} %copy.28.cum_row, f32[2,768]{1,0:T(2,128)} %copy.29.in_row, f32[768,2]{1,0:T(8,128)} %bitcast.55, bf16[768,256]{1,0:T(8,128)(2,1)} %query_ref.1, bf16[768,256]{1,0:T(8,128)(2,1)} %key_ref.1, ...), custom_call_target="tpu_custom_call" | custom-call | tf_op jit(solution)/shard_map/layer/pallas_call | solution.py:441
  213.7 2.1 copy.43
  (4 shorter events, 0.0 us)
Async XLA Ops:
  1.9 2.8 %copy-start = (f32[2,6,128]{0,2,1:T(8,128)}, f32[2,6,128]{0,2,1:T(8,128)S(1)}, u32[]{:S(2)}) copy-start(f32[2,6,128]{0,2,1:T(8,128)S(1)} %copy.23) | copy-start | bytes 18436
  2.8 2.1 copy-start.1
  3.8 2.3 %copy-start.2 = (bf16[768,512]{1,0:T(8,128)(2,1)S(1)}, bf16[768,512]{1,0:T(8,128)(2,1)}, u32[]{:S(2)}) copy-start(bf16[768,512]{1,0:T(8,128)(2,1)} %value_ref.1) | copy-start | bytes 2359300

commit v2 on v1

--- a/solution.py
+++ b/solution.py
@@ -243,9 +243,6 @@
                 )
 
     if carried_by_hand:
-        crossed(3, 0).wait_recv()
-        for way in (1, -1):
-            send_along(3, 0, other, False, way)
         stage(1, (0,))
 
     tile = rows_all // 3
@@ -303,7 +300,11 @@
     sent += spread(gated, blocks, gated_sems)
     blocks[me] = gated[...]
     if carried_by_hand:
-        stage(1, (1, 2, 3))
+        stage(1, (1, 2))
+        crossed(3, 0).wait_recv()
+        for way in (1, -1):
+            send_along(3, 0, other, False, way)
+        stage(1, (3,))
     sent += relay(weight, proj_sems)
     if carried_by_hand:
         stage(2, (0, 1))
@@ -332,7 +333,7 @@
 
     if carried_by_hand:
         stage(2, (2, 3))
-        stage(3, (0, 1))
+        stage(3, (0, 1, 2))
         finish((0, 1))
         own(0).wait()
         own(1).wait()
@@ -348,10 +349,9 @@
         active[rows, :] = (gate / (1.0 + jnp.exp(-gate)) * up).astype(jnp.bfloat16)
         return unused
 
-    if carried_by_hand:
-        stage(3, (2, 3))
     lax.fori_loop(0, 3, mix, 0)
     if carried_by_hand:
+        stage(3, (3,))
         finish((2, 3))
         own(2).wait()
         own(3).wait()

time: 216 us -> 219 us (1.014)
  Pallas kernels: 206 us -> 209 us
    pallas_call x1, Pallas kernels: 206 us -> 209 us  [layer(): pl.pallas_call(functools.partial(layer_kernel, ranks, count, heads, carri...]
where the time goes in v2:
time: 219 us
  Pallas kernels  209 us (95%)
  local copies, waits for them, and re-layouts  6.18 us (3%)
    pallas_call x1, Pallas kernels, layer(): pl.pallas_call(functools.partial(layer_kernel, ranks, count, heads, carri...  209 us

profile of v2, /device:TPU:25, one launch (start us, length us, event | category | flops | bytes accessed | tf_op | source)
XLA Modules:
  0.0 219.0 jit_solution(11031336934393075733)
XLA Ops:
  0.0 0.7 fusion.15
  0.8 0.6 reduce-window.6
  1.3 0.2 slice_reduce_fusion
  1.5 0.2 reduce-window.9
  1.7 0.1 broadcast_add_fusion
  1.8 0.2 copy.23
  1.9 0.0 copy-start
  2.0 0.1 pad.7.clone
  2.0 0.7 copy.28.cum_row
  2.8 0.0 copy-start.1
  2.8 0.9 copy.24
  3.7 0.1 fusion.12
  3.8 0.0 copy-start.2
  3.9 0.1 pad.6.clone
  3.9 0.7 copy.29.in_row
  4.7 0.1 subtract_exponential_fusion
  4.8 0.0 copy-done
  4.8 0.1 copy.30
  4.9 0.0 copy-done.1
  4.9 0.3 fusion.9
  5.2 0.1 broadcast_add_fusion.1
  5.3 0.1 maximum_maximum_fusion
  5.3 0.6 pad.4.aux_ref
  6.0 0.1 copy.25
  6.1 0.0 copy-done.2
  6.1 0.3 copy.32
  6.4 1.5 fusion.5
  7.9 209.0 %layer.1 = bf16[768,512]{1,0:T(8,128)(2,1)} custom-call(bf16[512,128]{1,0:T(8,128)(2,1)} %bitcast.59, f32[8,128]{1,0:T(8,128)} %pad.4.aux_ref, f32[2,768]{1,0:T(2,128)} %copy.28.cum_row, f32[2,768]{1,0:T(2,128)} %copy.29.in_row, f32[768,2]{1,0:T(8,128)} %bitcast.55, bf16[768,256]{1,0:T(8,128)(2,1)} %query_ref.1, bf16[768,256]{1,0:T(8,128)(2,1)} %key_ref.1, ...), custom_call_target="tpu_custom_call" | custom-call | tf_op jit(solution)/shard_map/layer/pallas_call | solution.py:441
  216.9 2.1 copy.43
  (4 shorter events, 0.0 us)
Async XLA Ops:
  1.9 2.8 %copy-start = (f32[2,6,128]{0,2,1:T(8,128)}, f32[2,6,128]{0,2,1:T(8,128)S(1)}, u32[]{:S(2)}) copy-start(f32[2,6,128]{0,2,1:T(8,128)S(1)} %copy.23) | copy-start | bytes 18436
  2.8 2.1 copy-start.1
  3.8 2.3 %copy-start.2 = (bf16[768,512]{1,0:T(8,128)(2,1)S(1)}, bf16[768,512]{1,0:T(8,128)(2,1)}, u32[]{:S(2)}) copy-start(bf16[768,512]{1,0:T(8,128)(2,1)} %value_ref.1) | copy-start | bytes 2359300

commit v3 on v1

--- a/solution.py
+++ b/solution.py
@@ -332,7 +332,7 @@
 
     if carried_by_hand:
         stage(2, (2, 3))
-        stage(3, (0, 1))
+        stage(3, (0, 1, 2))
         finish((0, 1))
         own(0).wait()
         own(1).wait()
@@ -348,10 +348,9 @@
         active[rows, :] = (gate / (1.0 + jnp.exp(-gate)) * up).astype(jnp.bfloat16)
         return unused
 
-    if carried_by_hand:
-        stage(3, (2, 3))
     lax.fori_loop(0, 3, mix, 0)
     if carried_by_hand:
+        stage(3, (3,))
         finish((2, 3))
         own(2).wait()
         own(3).wait()

time: 216 us -> 212 us (0.981)
  Pallas kernels: 206 us -> 202 us
    pallas_call x1, Pallas kernels: 206 us -> 202 us  [layer(): pl.pallas_call(functools.partial(layer_kernel, ranks, count, heads, carri...]
where the time goes in v3:
time: 212 us
  Pallas kernels  202 us (95%)
  local copies, waits for them, and re-layouts  6.18 us (3%)
    pallas_call x1, Pallas kernels, layer(): pl.pallas_call(functools.partial(layer_kernel, ranks, count, heads, carri...  202 us

profile of v3, /device:TPU:25, one launch (start us, length us, event | category | flops | bytes accessed | tf_op | source)
XLA Modules:
  0.0 211.9 jit_solution(3730808388254791454)
XLA Ops:
  0.0 0.7 fusion.15
  0.8 0.6 reduce-window.6
  1.3 0.2 slice_reduce_fusion
  1.5 0.2 reduce-window.9
  1.7 0.1 broadcast_add_fusion
  1.8 0.2 copy.23
  1.9 0.0 copy-start
  2.0 0.1 pad.7.clone
  2.0 0.7 copy.28.cum_row
  2.8 0.0 copy-start.1
  2.8 0.9 copy.24
  3.7 0.1 fusion.12
  3.8 0.0 copy-start.2
  3.9 0.1 pad.6.clone
  3.9 0.7 copy.29.in_row
  4.7 0.1 subtract_exponential_fusion
  4.8 0.0 copy-done
  4.8 0.1 copy.30
  4.9 0.0 copy-done.1
  4.9 0.3 fusion.9
  5.2 0.1 broadcast_add_fusion.1
  5.3 0.1 maximum_maximum_fusion
  5.3 0.6 pad.4.aux_ref
  6.0 0.1 copy.25
  6.1 0.0 copy-done.2
  6.1 0.3 copy.32
  6.4 1.5 fusion.5
  7.9 201.9 %layer.1 = bf16[768,512]{1,0:T(8,128)(2,1)} custom-call(bf16[512,128]{1,0:T(8,128)(2,1)} %bitcast.59, f32[8,128]{1,0:T(8,128)} %pad.4.aux_ref, f32[2,768]{1,0:T(2,128)} %copy.28.cum_row, f32[2,768]{1,0:T(2,128)} %copy.29.in_row, f32[768,2]{1,0:T(8,128)} %bitcast.55, bf16[768,256]{1,0:T(8,128)(2,1)} %query_ref.1, bf16[768,256]{1,0:T(8,128)(2,1)} %key_ref.1, ...), custom_call_target="tpu_custom_call" | custom-call | tf_op jit(solution)/shard_map/layer/pallas_call | solution.py:440
  209.9 2.1 copy.43
  (4 shorter events, 0.0 us)
Async XLA Ops:
  1.9 2.8 %copy-start = (f32[2,6,128]{0,2,1:T(8,128)}, f32[2,6,128]{0,2,1:T(8,128)S(1)}, u32[]{:S(2)}) copy-start(f32[2,6,128]{0,2,1:T(8,128)S(1)} %copy.23) | copy-start | bytes 18436
  2.8 2.1 %copy-start.1 = (bf16[768,256]{1,0:T(8,128)(2,1)S(1)}, bf16[768,256]{1,0:T(8,128)(2,1)}, u32[]{:S(2)}) copy-start(bf16[768,256]{1,0:T(8,128)(2,1)} %key_ref.1) | copy-start | bytes 1179652
  3.8 2.3 %copy-start.2 = (bf16[768,512]{1,0:T(8,128)(2,1)S(1)}, bf16[768,512]{1,0:T(8,128)(2,1)}, u32[]{:S(2)}) copy-start(bf16[768,512]{1,0:T(8,128)(2,1)} %value_ref.1) | copy-start | bytes 2359300
